TPU v7x, 32 devices: a whole 2x2x4 slice. The times are simulated.
32 devices in a mesh: sp: 4 (over y, x), tp: 8 (over z, core).
Axes of the slice: x: 2, y: 2, z: 4, core: 2. Of those that a mesh axis runs over, the one named last changes fastest.
Arguments:
- conv_value: bfloat16 [1024, 2048], P('tp', 'sp'), may hold values from -6 to 6
- conv_gate: bfloat16 [1024, 2048], P('tp', 'sp'), may hold values from -6 to 6
- conv_taps: float32 [1024, 31], P('tp'), may hold values from -2.2 to 2.2
- norm_gain: float32 [1024], replicated, may hold values from 0.1 to 1.9
- norm_bias: float32 [1024], replicated, may hold values from -3 to 3
- out_weight: bfloat16 [1024, 2048], replicated, may hold values from -0.1875 to 0.1875
- stream: bfloat16 [2048, 2048], P(('sp', 'tp')), may hold values from -6 to 6
- routes: int32 [2048, 2], P(('sp', 'tp')), may hold values from 0 to 3, all different within a row; in each aligned block of 64 rows (0 to 63, 64 to 127, ...) at most 32 rows name the same one
- route_weights: float32 [2048, 2], P(('sp', 'tp')), may hold values from 0.2 to 1
- expert_gain: float32 [2048], replicated, may hold values from 0.1 to 1.9
- expert_gate: bfloat16 [4, 2048, 7168], P('sp', None, 'tp'), may hold values from -0.125 to 0.125
- expert_up: bfloat16 [4, 2048, 7168], P('sp', None, 'tp'), may hold values from -0.125 to 0.125
- expert_down: bfloat16 [4, 7168, 2048], P('sp', 'tp'), may hold values from -0.0625 to 0.0625
Outputs:
- mixed: bfloat16 [2048, 2048], P(('sp', 'tp'))
Inputs may be any that keep to these rules, and one draw needn't show every extreme that they name: `routes`: within each device's 64 rows every expert is named exactly 32 times; a row names distinct experts.
All inputs are finite; a program needn't handle non-finite values.
Results may differ from a plain program's by a relative error of at most 0.014.
Values may be sent and summed in bfloat16 or wider, within the bound.
A program may use at most 64 MiB of HBM per device.

v0:
```python
import functools

import jax
import jax.numpy as jnp
from jax import lax
from jax.experimental import pallas as pl
from jax.experimental.pallas import tpu as pltpu
from jax.sharding import PartitionSpec as P

epsilon = 1e-06
MESH = pl.DeviceIdType.MESH
QUARTERS = 4


def shifted(value, axis, steps):
    count = lax.axis_size(axis)
    initial, last = (max(0, -steps), min(count, count - steps))
    return lax.ppermute(value, axis, [(source, source + steps) for source in range(initial, last)])


def moe_kernel(
    S,
    Z,
    C,
    packed,
    normed_ref,
    resid_ref,
    routes_ref,
    weights_ref,
    gate_hbm,
    up_hbm,
    down_hbm,
    out_ref,
    sendbuf,
    xbuf,
    wg,
    wu,
    wd,
    hid,
    mine,
    pout,
    pin,
    rbuf,
    fin,
    ret,
    w_sem,
    disp_send,
    disp_recv,
    agz_send,
    agz_recv,
    ags_send,
    ags_recv,
    rss_send,
    rss_recv,
    rsz_send,
    rsz_recv,
    ret_send,
    ret_recv,
):
    f32, bf16 = jnp.float32, jnp.bfloat16
    s_me = lax.axis_index("sp")
    t_me = lax.axis_index("tp")
    z_me, c_me = t_me // 2, t_me % 2
    half = Z // 2
    Q = S // QUARTERS
    W = normed_ref.shape[1]
    tokens = normed_ref.shape[0]
    F = down_hbm.shape[1]
    QR = Q * C
    M = Z * 2 * QR

    def sp_peer(steps):
        return (lax.rem(s_me + steps + S, S), t_me)

    def z_peer(steps):
        return (s_me, lax.rem(z_me + steps + Z, Z) * 2 + c_me)

    sibling = (s_me, z_me * 2 + 1 - c_me)

    loads = []
    if packed:
        tiles = F // 128
        for j in range(tiles):
            for k, src in enumerate((gate_hbm, up_hbm)):
                loads.append(
                    pltpu.make_async_copy(
                        src.at[0, :, pl.ds(j * 128, 128)],
                        wg.at[j, :, pl.ds(k * 128, 128)],
                        w_sem.at[2 * j + k],
                    )
                )
    else:
        tiles = 1
        loads.append(pltpu.make_async_copy(gate_hbm.at[0], wg.at[0], w_sem.at[0]))
        loads.append(pltpu.make_async_copy(up_hbm.at[0], wu.at[0], w_sem.at[1]))
    down_load = pltpu.make_async_copy(down_hbm.at[0], wd, w_sem.at[2 * tiles])
    for cp in loads:
        cp.start()
    down_load.start()

    barrier = pltpu.get_barrier_semaphore()
    peers = [sp_peer(j) for j in range(1, S)] + [z_peer(1), z_peer(-1), sibling]
    for peer in peers:
        pl.semaphore_signal(barrier, inc=1, device_id=peer, device_id_type=MESH)

    r0, r1 = routes_ref[0:1, :], routes_ref[1:2, :]
    w0, w1 = weights_ref[0:1, :], weights_ref[1:2, :]
    ids = s_me - lax.broadcasted_iota(jnp.int32, (S, tokens), 0)
    ids = jnp.where(ids < 0, ids + S, ids)
    hit0, hit1 = r0 == ids, r1 == ids
    named = jnp.where(hit0 | hit1, 1.0, 0.0)
    row_w = jnp.where(hit0, w0, 0.0) + jnp.where(hit1, w1, 0.0)
    earlier = jnp.where(
        lax.broadcasted_iota(jnp.int32, (tokens, tokens), 0)
        < lax.broadcasted_iota(jnp.int32, (tokens, tokens), 1),
        1.0,
        0.0,
    )
    rank = jnp.dot(named.astype(bf16), earlier.astype(bf16), preferred_element_type=f32)
    slot = lax.broadcasted_iota(jnp.int32, (C, tokens), 0).astype(f32)
    choose, weigh = [], []
    for j in range(S):
        pick = jnp.where(rank[j : j + 1, :] == slot, named[j : j + 1, :], 0.0)
        choose.append(pick)
        weigh.append(pick * row_w[j : j + 1, :])
    rows = normed_ref[...]
    sent = jnp.dot(
        jnp.concatenate(choose, axis=0).astype(bf16), rows, preferred_element_type=f32
    ).astype(bf16)
    xbuf[0, 0, 0, 0] = sent[0:C]
    for j in range(1, S):
        sendbuf[j] = sent[j * C : (j + 1) * C]

    pl.semaphore_wait(barrier, len(peers))

    sends = []

    def remote(src, dst, send_sem, recv_sem, peer):
        return pltpu.make_async_remote_copy(
            src_ref=src,
            dst_ref=dst,
            send_sem=send_sem,
            recv_sem=recv_sem,
            device_id=peer,
            device_id_type=MESH,
        )

    def start(cp):
        cp.start()
        sends.append(cp)

    def disp(j):
        return remote(
            sendbuf.at[j],
            xbuf.at[j // Q, 0, 0, j % Q],
            disp_send.at[j],
            disp_recv.at[j],
            sp_peer(-j),
        )

    def sign(d):
        return 1 if d == 0 else -1

    def reach(d, q):
        return half if d == q % 2 else half - 1

    def agz(d, k, q):
        return remote(
            xbuf.at[q, (-sign(d) * (k - 1)) % Z, 0],
            xbuf.at[q, (-sign(d) * k) % Z, 0],
            agz_send.at[d, k - 1, q],
            agz_recv.at[d, k - 1, q],
            z_peer(sign(d)),
        )

    def ags(q, r):
        return remote(
            xbuf.at[q, r, 0], xbuf.at[q, r, 1], ags_send.at[q, r], ags_recv.at[q, r], sibling
        )

    def rss(q, r):
        return remote(
            pout.at[q, r], pin.at[q, r], rss_send.at[q, r], rss_recv.at[q, r], sibling
        )

    def rsz(d, k, q):
        return remote(
            mine.at[q, (sign(d) * k) % Z],
            rbuf.at[d, k - 1, q],
            rsz_send.at[d, k - 1, q],
            rsz_recv.at[d, k - 1, q],
            z_peer(sign(d)),
        )

    def back(j):
        return remote(
            fin.at[j // Q, j % Q], ret.at[j], ret_send.at[j], ret_recv.at[j], sp_peer(j)
        )

    def first_hop(q):
        for i in range(Q):
            j = q * Q + i
            if j > 0:
                disp(j).wait_recv()
        for d in (q % 2, 1 - q % 2):
            if reach(d, q) >= 1:
                start(agz(d, 1, q))
        start(ags(q, 0))

    def forward(q, k):
        for d in (q % 2, 1 - q % 2):
            if reach(d, q) >= k:
                agz(d, k, q).wait_recv()
                if k < reach(d, q):
                    start(agz(d, k + 1, q))
                start(ags(q, (-sign(d) * k) % Z))

    def ready(q):
        for r in range(Z):
            ags(q, r).wait_recv()

    def ffn_up(q):
        if q == 0:
            for cp in loads:
                cp.wait()

        def tile(j, carry):
            x = xbuf[q].reshape(M, W)
            if packed:
                both = jnp.dot(x, wg[j], preferred_element_type=f32)
                g, u = both[:, :128], both[:, 128:]
                hid[:, pl.ds(pl.multiple_of(j * 128, 128), 128)] = (jax.nn.silu(g) * u).astype(bf16)
            else:
                g = jnp.dot(x, wg[0], preferred_element_type=f32)
                u = jnp.dot(x, wu[0], preferred_element_type=f32)
                hid[...] = (jax.nn.silu(g) * u).astype(bf16)
            return carry

        lax.fori_loop(0, tiles, tile, 0, unroll=True)

    step = 512

    def ffn_down(q):
        if q == 0:
            down_load.wait()

        def tile(n, carry):
            cols = pl.ds(pl.multiple_of(n * step, step), step)
            y = jnp.dot(hid[...], wd[:, cols], preferred_element_type=f32).astype(bf16)
            y = y.reshape(Z, 2, QR, step)
            mine[q, :, :, cols] = y[:, 0]
            pout[q, :, :, cols] = y[:, 1]
            return carry

        lax.fori_loop(0, W // step, tile, 0, unroll=True)
        for k in range(half, 0, -1):
            for r in sorted({k % Z, -k % Z}):
                start(rss(q, r))
        start(rss(q, 0))

    def pair_sum(q, r, extra=None):
        rss(q, r).wait_recv()
        total = mine[q, r].astype(f32) + pin[q, r].astype(f32)
        if extra is not None:
            total = total + extra[...].astype(f32)
        mine[q, r] = total.astype(bf16)

    def launch(q):
        for k in range(half, 0, -1):
            for d in (q % 2, 1 - q % 2):
                if reach(d, q) == k:
                    pair_sum(q, (sign(d) * k) % Z)
                    start(rsz(d, k, q))

    def relay(q):
        for k in range(half - 1, 0, -1):
            for d in (q % 2, 1 - q % 2):
                if reach(d, q) > k:
                    rsz(d, k + 1, q).wait_recv()
                    pair_sum(q, (sign(d) * k) % Z, rbuf.at[d, k, q])
                    start(rsz(d, k, q))

    def finish(q):
        rss(q, 0).wait_recv()
        total = mine[q, 0].astype(f32) + pin[q, 0].astype(f32)
        for d in (0, 1):
            if reach(d, q) >= 1:
                rsz(d, 1, q).wait_recv()
                total = total + rbuf[d, 0, q].astype(f32)
        done = total.astype(bf16).reshape(Q, C, W)
        if q == 0:
            ret[0] = done[0]
        fin[q] = done
        for i in range(Q):
            j = q * Q + i
            if j > 0:
                start(back(j))

    def far(f, q):
        for k in range(2, half + 1):
            f(q, k)

    for j in range(1, S):
        start(disp(j))
    first_hop(0)
    first_hop(1)
    forward(0, 1)
    first_hop(2)
    forward(1, 1)
    first_hop(3)
    far(forward, 0)
    ready(0)
    ffn_up(0)
    forward(2, 1)
    far(forward, 1)
    ffn_down(0)
    forward(3, 1)
    ready(1)
    launch(0)
    ffn_up(1)
    far(forward, 2)
    ffn_down(1)
    relay(0)
    far(forward, 3)
    ready(2)
    launch(1)
    ffn_up(2)
    ffn_down(2)
    relay(1)
    ready(3)
    launch(2)
    ffn_up(3)
    finish(0)
    ffn_down(3)
    relay(2)
    launch(3)
    finish(1)
    relay(3)
    finish(2)
    finish(3)

    spread = jnp.concatenate(weigh, axis=0).T
    high = spread.astype(bf16)
    low = (spread - high.astype(f32)).astype(bf16)
    for j in range(1, S):
        back(j).wait_recv()
    got = ret[...].reshape(S * C, W)
    mix = jnp.dot(high, got, preferred_element_type=f32) + jnp.dot(
        low, got, preferred_element_type=f32
    )
    out_ref[...] = (resid_ref[...].astype(f32) + mix).astype(bf16)
    for cp in sends:
        cp.wait_send()


def routed_experts(normed, residual, routes, route_weights, gate_w, up_w, down_w):
    S, T = lax.axis_size("sp"), lax.axis_size("tp")
    Z, half = T // 2, T // 4
    tokens, W = normed.shape
    C = routes.shape[1] * tokens // S
    Q = S // QUARTERS
    F = gate_w.shape[2]
    packed = F % 128 == 0
    tiles = F // 128 if packed else 1
    M = Z * 2 * Q * C
    bf16 = jnp.bfloat16
    vmem = pl.BlockSpec(memory_space=pltpu.VMEM)
    hbm = pl.BlockSpec(memory_space=pl.ANY)
    dma = pltpu.SemaphoreType.DMA
    quarter = (Q * C, W)
    return pl.pallas_call(
        functools.partial(moe_kernel, S, Z, C, packed),
        out_shape=jax.ShapeDtypeStruct((tokens, W), bf16),
        in_specs=[vmem] * 4 + [hbm] * 3,
        out_specs=vmem,
        scratch_shapes=[
            pltpu.VMEM((S, C, W), bf16),
            pltpu.VMEM((QUARTERS, Z, 2, Q, C, W), bf16),
            pltpu.VMEM((tiles, W, 256) if packed else (1, W, F), bf16),
            pltpu.VMEM((1, 16, 128) if packed else (1, W, F), bf16),
            pltpu.VMEM((F, W), bf16),
            pltpu.VMEM((M, F), bf16),
            pltpu.VMEM((QUARTERS, Z) + quarter, bf16),
            pltpu.VMEM((QUARTERS, Z) + quarter, bf16),
            pltpu.VMEM((QUARTERS, Z) + quarter, bf16),
            pltpu.VMEM((2, half, QUARTERS) + quarter, bf16),
            pltpu.VMEM((QUARTERS, Q, C, W), bf16),
            pltpu.VMEM((S, C, W), bf16),
            dma((2 * tiles + 1,)),
            dma((S,)),
            dma((S,)),
            dma((2, half, QUARTERS)),
            dma((2, half, QUARTERS)),
            dma((QUARTERS, Z)),
            dma((QUARTERS, Z)),
            dma((QUARTERS, Z)),
            dma((QUARTERS, Z)),
            dma((2, half, QUARTERS)),
            dma((2, half, QUARTERS)),
            dma((S,)),
            dma((S,)),
        ],
        compiler_params=pltpu.CompilerParams(
            collective_id=0, has_side_effects=True, vmem_limit_bytes=56 * 1024 * 1024
        ),
        name="routed_experts",
    )(normed, residual, routes.T, route_weights.T, gate_w, up_w, down_w)


def exchange_kernel(T, blocks_ref, out_ref, land, send_sem, recv_sem):
    s_me = lax.axis_index("sp")
    t_me = lax.axis_index("tp")
    barrier = pltpu.get_barrier_semaphore()
    for i in range(1, T):
        peer = (s_me, lax.rem(t_me + i, T))
        pl.semaphore_signal(barrier, inc=1, device_id=peer, device_id_type=MESH)
    pl.semaphore_wait(barrier, T - 1)
    copies = []
    for i in range(1, T):
        target = lax.rem(t_me + i, T)
        copies.append(
            pltpu.make_async_remote_copy(
                src_ref=blocks_ref.at[target],
                dst_ref=land.at[t_me],
                send_sem=send_sem.at[i],
                recv_sem=recv_sem.at[i],
                device_id=(s_me, target),
                device_id_type=MESH,
            )
        )
    for cp in copies:
        cp.start()
    land[t_me] = blocks_ref[t_me]
    for cp in copies:
        cp.wait()
    out_ref[...] = land[...]


def exchange(blocks):
    T = blocks.shape[0]
    vmem = pl.BlockSpec(memory_space=pltpu.VMEM)
    return pl.pallas_call(
        functools.partial(exchange_kernel, T),
        out_shape=jax.ShapeDtypeStruct(blocks.shape, blocks.dtype),
        in_specs=[vmem],
        out_specs=vmem,
        scratch_shapes=[
            pltpu.VMEM(blocks.shape, blocks.dtype),
            pltpu.SemaphoreType.DMA((T,)),
            pltpu.SemaphoreType.DMA((T,)),
        ],
        compiler_params=pltpu.CompilerParams(collective_id=1, has_side_effects=True),
        name="exchange",
    )(blocks)


def per_device(
    conv_value,
    conv_gate,
    conv_taps,
    norm_gain,
    norm_bias,
    out_weight,
    stream,
    routes,
    route_weights,
    expert_gain,
    expert_gate,
    expert_up,
    expert_down,
):
    f32 = jnp.float32
    local_ch = conv_value.shape[0]
    run_len = conv_value.shape[1]
    kernel_len = conv_taps.shape[1]
    gated_input = (conv_value.astype(f32) * jax.nn.sigmoid(conv_gate.astype(f32))).astype(
        jnp.bfloat16
    )
    left_rim = shifted(gated_input[:, run_len - (kernel_len - 1) :], "sp", 1)
    padded = jnp.concatenate([left_rim, gated_input], axis=1).astype(f32)
    conv_sum = jnp.zeros((local_ch, run_len), f32)
    for offset in range(kernel_len):
        conv_sum = (
            conv_sum + conv_taps[:, offset : offset + 1] * padded[:, offset : offset + run_len]
        )
    conv_out = conv_sum.astype(jnp.bfloat16)
    parts = lax.axis_size("tp")
    tok_rows = run_len // parts
    pieces = exchange(conv_out.T.reshape(parts, tok_rows, local_ch))
    whole_conv = pieces.transpose(1, 0, 2).reshape(tok_rows, parts * local_ch).astype(f32)
    center = jnp.mean(whole_conv, axis=1, keepdims=True)
    spread = jnp.mean((whole_conv - center) ** 2, axis=1, keepdims=True)
    scaled = (whole_conv - center) * lax.rsqrt(spread + epsilon) * norm_gain + norm_bias
    token_major = jax.nn.silu(scaled).astype(jnp.bfloat16)
    projected = jnp.dot(token_major, out_weight, preferred_element_type=f32)
    residual = (stream.astype(f32) + projected).astype(jnp.bfloat16)
    res_float = residual.astype(f32)
    normed = (
        res_float
        * lax.rsqrt(jnp.mean(res_float * res_float, axis=1, keepdims=True) + epsilon)
        * expert_gain
    ).astype(jnp.bfloat16)
    return routed_experts(
        normed, residual, routes, route_weights, expert_gate, expert_up, expert_down
    )


def solution(mesh):
    return jax.shard_map(
        per_device,
        mesh=mesh,
        in_specs=(
            P("tp", "sp"),
            P("tp", "sp"),
            P("tp", None),
            P(),
            P(),
            P(),
            P(("sp", "tp"), None),
            P(("sp", "tp"), None),
            P(("sp", "tp"), None),
            P(),
            P("sp", None, "tp"),
            P("sp", None, "tp"),
            P("sp", "tp", None),
        ),
        out_specs=P(("sp", "tp"), None),
        check_vma=False,
    )
```

profile of v0, /device:TPU:0, one launch (start us, length us, event | category | flops | bytes accessed | tf_op | source)
XLA Modules:
  0.0 113.6 jit_solution(11650559328667195787)
XLA Ops:
  0.0 1.0 multiply_convert_fusion.1
  1.0 0.1 slice.252
  1.1 4.9 %collective-permute-start = (bf16[128,30]{1,0:T(8,128)(2,1)S(1)}, bf16[128,30]{1,0:T(8,128)(2,1)S(1)}, u32[]{:S(2)}, u32[]{:S(2)}) collective-permute-start(bf16[128,30]{1,0:T(8,128)(2,1)S(1)} %slice.252), channel_id=1, source_target_pairs={{0,8},{8,16},{16,24},{1,9},{9,17},{17,25},{2,10},{10,18},{18,26},{... | collective-permute-start | bytes 23048 | tf_op jit(solution)/shard_map/ppermute | solution.py:18
  6.0 1.0 slice_bitcast_fusion.30
  7.0 1.0 slice_bitcast_fusion.29
  8.0 0.0 collective-permute-done
  8.0 0.1 maximum_convert_fusion
  8.1 0.0 copy-start.2
  8.1 0.0 copy-start.3
  8.1 0.0 copy-start.4
  8.1 3.0 %fusion.45 = bf16[512,128]{0,1:T(8,128)(2,1)S(1)} fusion(f32[128,542]{1,0:T(8,128)S(1)} %maximum_convert_fusion, f32[128]{0:T(128)S(1)} %get-tuple-element.34, f32[128]{0:T(128)S(1)} %get-tuple-element.35, f32[128]{0:T(128)S(1)} %get-tuple-element.6, f32[128]{0:T(128)S(1)} %get-tuple-element.7, f32[128]{0:T(128)S(1)} %get-tuple-element.8, ...), kind=kLoop, calls=%fused_computation.86 | loop fusion | flops 4063232 | bytes 8273408 | tf_op jit(solution)/shard_map/transpose | solution.py:489
  11.2 0.0 copy-start.1
  11.2 0.8 copy.15
  11.9 8.5 %exchange.1 = bf16[8,64,128]{2,1,0:T(8,128)(2,1)} custom-call(bf16[8,64,128]{2,1,0:T(8,128)(2,1)} %bitcast.86), custom_call_target="tpu_custom_call" | custom-call | tf_op jit(solution)/shard_map/exchange/pallas_call | solution.py:442
  20.5 1.0 convert_reduce_fusion
  21.5 1.1 fusion.5
  22.6 0.0 copy-done.2
  22.7 0.0 copy-done.3
  22.7 0.0 copy-done.4
  22.7 3.4 %fusion.1 = (f32[64]{0:T(128)S(1)}, bf16[64,2048]{1,0:T(8,128)(2,1)S(1)}) fusion(bf16[1024,2048]{1,0:T(8,128)(2,1)} %param.18, f32[1024]{0:T(1024)S(1)} %copy-done.3, f32[1024]{0:T(1024)S(1)} %copy-done.4, f32[64]{0:T(128)S(1)} %add_rsqrt_fusion.1, f32[64]{0:T(128)S(1)} %broadcast_multiply_fusion, bf16[64,2048]{1,0:T(8,128)(2,1)S(1)} %copy-done.2, ...), kind=kOutput, calls=%fused_computation.4 | convolution fusion | flops 269877184 | bytes 4858624 | tf_op jit(solution)/shard_map/dot_general | solution.py:495
  26.0 0.0 copy-start
  26.1 0.0 copy-done.1
  26.1 0.8 fusion.3.normed_ref
  26.9 0.0 copy-done
  26.9 85.0 %routed_experts.1 = bf16[64,2048]{1,0:T(8,128)(2,1)} custom-call(bf16[64,2048]{1,0:T(8,128)(2,1)} %fusion.3.normed_ref, bf16[64,2048]{1,0:T(8,128)(2,1)} %copy-done, s32[2,64]{1,0:T(2,128)} %bitcast.87, f32[2,64]{1,0:T(2,128)} %bitcast.88, bf16[1,2048,896]{2,1,0:T(8,128)(2,1)} %gate_hbm.1, bf16[1,2048,896]{2,1,0:T(8,128)(2,1)} %up_hbm.1, ...), custom_call_target="tpu_custom_call" | custom-call | tf_op jit(solution)/shard_map/routed_experts/pallas_call | solution.py:371
  111.9 1.7 %copy.25 = bf16[64,2048]{1,0:T(8,128)(2,1)} copy(bf16[64,2048]{1,0:T(8,128)(2,1)} %routed_experts.1) | data formatting | bytes 524288
  (3 shorter events, 0.0 us)
Async XLA Ops:
  1.1 6.8 %collective-permute-start = (bf16[128,30]{1,0:T(8,128)(2,1)S(1)}, bf16[128,30]{1,0:T(8,128)(2,1)S(1)}, u32[]{:S(2)}, u32[]{:S(2)}) collective-permute-start(bf16[128,30]{1,0:T(8,128)(2,1)S(1)} %slice.252), channel_id=1, source_target_pairs={{0,8},{8,16},{16,24},{1,9},{9,17},{17,25},{2,10},{10,18},{18,26},{... | collective-permute-start | bytes 23048 | tf_op jit(solution)/shard_map/ppermute | solution.py:18
  8.1 14.5 %copy-start.2 = (bf16[64,2048]{1,0:T(8,128)(2,1)S(1)}, bf16[64,2048]{1,0:T(8,128)(2,1)}, u32[]{:S(2)}) copy-start(bf16[64,2048]{1,0:T(8,128)(2,1)} %param.19) | copy-start | bytes 786436
  8.1 14.5 %copy-start.3 = (f32[1024]{0:T(1024)S(1)}, f32[1024]{0:T(1024)}, u32[]{:S(2)}) copy-start(f32[1024]{0:T(1024)} %param.17) | copy-start | bytes 12292
  8.1 14.5 %copy-start.4 = (f32[1024]{0:T(1024)S(1)}, f32[1024]{0:T(1024)}, u32[]{:S(2)}) copy-start(f32[1024]{0:T(1024)} %param.16) | copy-start | bytes 12292
  11.2 14.9 %copy-start.1 = (f32[2048]{0:T(1024)S(1)}, f32[2048]{0:T(1024)}, u32[]{:S(2)}) copy-start(f32[2048]{0:T(1024)} %param.22) | copy-start | bytes 24580
  26.0 0.9 copy-start
where the time goes:
time: 114 us
  Pallas kernels  93.5 us (82%)
  other arithmetic  7.15 us (6%)
  starting transfers between devices  4.86 us (4%)
  local copies, waits for them, and re-layouts  4.5 us (4%)
  matrix products  3.37 us (3%)
    pallas_call x1, Pallas kernels, routed_experts(): pl.pallas_call(functools.partial(moe_kernel, S, Z, C, packed), out_shape=...  85 us
    pallas_call x1, Pallas kernels, exchange(): pl.pallas_call(functools.partial(exchange_kernel, T), out_shape=jax.Shape...  8.53 us
    ppermute x1, starting transfers between devices, shifted(): lax.ppermute(value, axis, [(source, source + steps) for source in range(i...  4.86 us
    dot_general x1, matrix products, per_device(): projected = jnp.dot(token_major, out_weight, preferred_element_type=f32)  3.37 us
    transpose x1, other arithmetic, per_device(): pieces = exchange(conv_out.T.reshape(parts, tok_rows, local_ch))  3.01 us
  transfers between devices with their start and end apart: 1, of which 0 were waited for; matrix products, arithmetic and copies ran while one was open for 2% of the time, Pallas kernels for 0%

commit v1 on v0

--- a/solution.py
+++ b/solution.py
@@ -454,6 +454,519 @@
     )(blocks)
 
 
+class Link:
+    def __init__(self):
+        self.sent = []
+
+    def copy(self, src, dst, send_sem, recv_sem, peer):
+        return pltpu.make_async_remote_copy(
+            src_ref=src,
+            dst_ref=dst,
+            send_sem=send_sem,
+            recv_sem=recv_sem,
+            device_id=peer,
+            device_id_type=MESH,
+        )
+
+    def start(self, cp, cond=None):
+        self.sent.append((cp, cond))
+        if cond is None:
+            cp.start()
+        else:
+            pl.when(cond)(cp.start)
+
+    def drain(self):
+        for cp, cond in self.sent:
+            if cond is None:
+                cp.wait_send()
+            else:
+                pl.when(cond)(cp.wait_send)
+
+
+def fused_kernel(
+    T,
+    C,
+    taps_n,
+    value_ref,
+    vgate_ref,
+    taps_ref,
+    gain_ref,
+    bias_ref,
+    routes_ref,
+    weights_ref,
+    egain_ref,
+    stream_ref,
+    outw_hbm,
+    gate_hbm,
+    up_hbm,
+    down_hbm,
+    out_ref,
+    gbuf,
+    halo_out,
+    halo_in,
+    cbuf,
+    land,
+    outw,
+    res,
+    meta,
+    cho,
+    hi,
+    lo,
+    tok,
+    sbuf,
+    X,
+    wg,
+    wd,
+    hid,
+    mine,
+    pout,
+    pin,
+    ret,
+    tot,
+    tout,
+    tin,
+    w_sem,
+    halo_sem,
+    ex_send,
+    ex_recv,
+    meta_send,
+    meta_recv,
+    tz_send,
+    tz_recv,
+    pl_send,
+    pl_recv,
+    sx_send,
+    sx_recv,
+    sy_send,
+    sy_recv,
+    rt_send,
+    rt_recv,
+    zo_send,
+    zo_recv,
+):
+    f32, bf16 = jnp.float32, jnp.bfloat16
+    s = lax.axis_index("sp")
+    t = lax.axis_index("tp")
+    z, c = t // 2, t % 2
+    Z, J = T // 2, 4
+    gy, gx = s // 2, s % 2
+    W = out_ref.shape[1]
+    tokens = out_ref.shape[0]
+    F = wd.shape[0]
+    tiles = F // 128
+    ch, run = value_ref.shape
+    rim = gbuf.shape[0] - run
+    link = Link()
+
+    def plane(j):
+        return (lax.rem(gy + j // 2, 2) * 2 + lax.rem(gx + j % 2, 2), t)
+
+    def at_z(zt):
+        return (s, zt * 2 + c)
+
+    sibling = (s, z * 2 + 1 - c)
+
+    zp = [z, 1 + z % 2, 2 + z // 2 - 2 * (z % 2), 3 - 3 * (z // 2)]
+
+    outw_load = pltpu.make_async_copy(outw_hbm, outw, w_sem.at[2 * tiles + 1])
+    outw_load.start()
+    loads = []
+    for j in range(tiles):
+        for k, src in enumerate((gate_hbm, up_hbm)):
+            loads.append(
+                pltpu.make_async_copy(
+                    src.at[0, :, pl.ds(j * 128, 128)],
+                    wg.at[j, :, pl.ds(k * 128, 128)],
+                    w_sem.at[2 * j + k],
+                )
+            )
+    down_load = pltpu.make_async_copy(down_hbm.at[0], wd, w_sem.at[2 * tiles])
+    for cp in loads:
+        cp.start()
+    down_load.start()
+
+    barrier = pltpu.get_barrier_semaphore()
+    peers = [plane(j) for j in range(1, J)] + [(s, lax.rem(t + i, T)) for i in range(1, T)]
+    for peer in peers:
+        pl.semaphore_signal(barrier, inc=1, device_id=peer, device_id_type=MESH)
+
+    gated = (
+        value_ref[...].astype(f32) * jax.nn.sigmoid(vgate_ref[...].astype(f32))
+    ).astype(bf16)
+    turned = gated.astype(f32).T
+    gbuf[rim:, :] = turned
+    halo_out[...] = turned[run - rim :, :].astype(bf16)
+    meta[z, 0:2, 0:tokens] = routes_ref[...].astype(f32)
+    meta[z, 2:4, 0:tokens] = weights_ref[...]
+
+    pl.semaphore_wait(barrier, len(peers))
+
+    S = J
+    halo = link.copy(
+        halo_out, halo_in, halo_sem.at[0], halo_sem.at[1], (lax.rem(s + 1, S), t)
+    )
+    link.start(halo, s < S - 1)
+
+    def mz(i, zs):
+        return link.copy(
+            meta.at[z], meta.at[z], meta_send.at[i - 1], meta_recv.at[z], at_z(zs)
+        )
+
+    for i in range(1, Z):
+        link.start(mz(i, lax.rem(z + i, Z)))
+
+    def conv(b):
+        acc = jnp.zeros((tokens, ch), f32)
+        for j in range(taps_n):
+            lead = rim - (taps_n - 1) + b * tokens + j
+            acc = acc + taps_ref[j : j + 1, :] * gbuf[lead : lead + tokens, :]
+        cbuf[b] = acc.astype(bf16)
+
+    for b in range(1, T):
+        conv(b)
+
+    @pl.when(s > 0)
+    def _():
+        halo.wait_recv()
+        gbuf[0:rim, :] = halo_in[...].astype(f32)
+
+    @pl.when(s == 0)
+    def _():
+        gbuf[0:rim, :] = jnp.zeros((rim, ch), f32)
+
+    conv(0)
+
+    exchanges = []
+    for i in range(1, T):
+        target = lax.rem(t + i, T)
+        cp = link.copy(
+            cbuf.at[target], land.at[t], ex_send.at[i - 1], ex_recv.at[i - 1], (s, target)
+        )
+        link.start(cp)
+        exchanges.append(cp)
+    land[t] = cbuf[t]
+
+    for i in range(1, Z):
+        zs = lax.rem(z + Z - i, Z)
+        link.copy(
+            meta.at[zs], meta.at[zs], meta_send.at[i - 1], meta_recv.at[zs], at_z(zs)
+        ).wait_recv()
+
+    row = lax.broadcasted_iota(jnp.int32, (J, tokens), 0)
+    ids = (((gy + (row >> 1)) & 1) * 2 + ((gx + (row & 1)) & 1)).astype(f32)
+    earlier = jnp.where(
+        lax.broadcasted_iota(jnp.int32, (tokens, tokens), 0)
+        < lax.broadcasted_iota(jnp.int32, (tokens, tokens), 1),
+        1.0,
+        0.0,
+    ).astype(bf16)
+    slot = lax.broadcasted_iota(jnp.int32, (C, tokens), 0).astype(f32)
+    for p in range(Z):
+        m = meta[zp[p]]
+        r0, r1 = m[0:1, :tokens], m[1:2, :tokens]
+        w0, w1 = m[2:3, :tokens], m[3:4, :tokens]
+        hit0, hit1 = r0 == ids, r1 == ids
+        named = jnp.where(hit0 | hit1, 1.0, 0.0)
+        row_w = jnp.where(hit0, w0, 0.0) + jnp.where(hit1, w1, 0.0)
+        rank = jnp.dot(named.astype(bf16), earlier, preferred_element_type=f32)
+        choose, weigh = [], []
+        for j in range(J):
+            pick = jnp.where(rank[j : j + 1, :] == slot, named[j : j + 1, :], 0.0)
+            choose.append(pick)
+            weigh.append(pick * row_w[j : j + 1, :])
+        cho[p] = jnp.concatenate(choose, axis=0).astype(bf16)
+        spread = jnp.concatenate(weigh, axis=0).T
+        high = spread.astype(bf16)
+        hi[p] = high
+        lo[p] = (spread - high.astype(f32)).astype(bf16)
+
+    for cp in exchanges:
+        cp.wait_recv()
+    whole = jnp.concatenate([land[i] for i in range(T)], axis=1).astype(f32)
+    center = jnp.mean(whole, axis=1, keepdims=True)
+    whole = whole - center
+    var = jnp.mean(whole * whole, axis=1, keepdims=True)
+    act = jax.nn.silu(
+        whole * lax.rsqrt(var + epsilon) * gain_ref[...] + bias_ref[...]
+    ).astype(bf16)
+    outw_load.wait()
+    step = 512
+    square = jnp.zeros((tokens, 1), f32)
+    for n in range(W // step):
+        cut = slice(n * step, (n + 1) * step)
+        r = (
+            stream_ref[:, cut].astype(f32)
+            + jnp.dot(act, outw[:, cut], preferred_element_type=f32)
+        ).astype(bf16)
+        res[:, cut] = r
+        rf = r.astype(f32)
+        square = square + jnp.sum(rf * rf, axis=1, keepdims=True)
+    scale = lax.rsqrt(square * (1.0 / W) + epsilon)
+    for n in range(W // step):
+        cut = slice(n * step, (n + 1) * step)
+        tok[z, :, cut] = (res[:, cut].astype(f32) * scale * egain_ref[:, cut]).astype(bf16)
+
+    def sign(d):
+        return 1 if d == 0 else -1
+
+    def inside(v):
+        return (v >= 0) & (v < Z)
+
+    def tz(d, k):
+        block = lax.rem(z - sign(d) * (k - 1) + Z, Z)
+        return link.copy(
+            tok.at[block],
+            tok.at[block],
+            tz_send.at[d, k - 1],
+            tz_recv.at[d, k - 1],
+            at_z(lax.rem(z + sign(d) + Z, Z)),
+        )
+
+    def tz_in(d, k):
+        block = lax.rem(z - sign(d) * k + Z, Z)
+        return link.copy(
+            tok.at[block],
+            tok.at[block],
+            tz_send.at[d, k - 1],
+            tz_recv.at[d, k - 1],
+            at_z(lax.rem(z + sign(d) + Z, Z)),
+        )
+
+    def arrive(k):
+        for d in (0, 1):
+            sg = sign(d)
+            pl.when(inside(z - sg * k))(tz_in(d, k).wait_recv)
+            if k < Z - 1:
+                link.start(tz(d, k + 1), inside(z - sg * k) & inside(z + sg))
+
+    def pland(p, j):
+        return link.copy(
+            sbuf.at[p, j - 1], X.at[p, j, 0], pl_send.at[p, j - 1], pl_recv.at[p, j - 1], plane(j)
+        )
+
+    def sibx(p, j):
+        return link.copy(X.at[p, j, 0], X.at[p, j, 1], sx_send.at[p, j], sx_recv.at[p, j], sibling)
+
+    def select(p):
+        for n in range(W // step):
+            cut = slice(n * step, (n + 1) * step)
+            sel = jnp.dot(cho[p], tok[zp[p], :, cut], preferred_element_type=f32).astype(bf16)
+            X[p, 0, 0, :, cut] = sel[0:C]
+            for j in range(1, J):
+                sbuf[p, j - 1, :, cut] = sel[j * C : (j + 1) * C]
+        for j in (3, 1, 2):
+            link.start(pland(p, j))
+        link.start(sibx(p, 0))
+
+    def gather(p):
+        for j in (3, 1, 2):
+            pland(p, j).wait_recv()
+            link.start(sibx(p, j))
+        for j in range(J):
+            sibx(p, j).wait_recv()
+
+    M = J * 2 * C
+
+    def ffn_up(p):
+        if p == 0:
+            for cp in loads:
+                cp.wait()
+        for j in range(tiles):
+            x = X[p].reshape(M, W)
+            both = jnp.dot(x, wg[j], preferred_element_type=f32)
+            g, u = both[:, :128], both[:, 128:]
+            hid[:, j * 128 : (j + 1) * 128] = (jax.nn.silu(g) * u).astype(bf16)
+
+    H = pout.shape[0]
+    span = W // H
+
+    def siby(p, h):
+        return link.copy(
+            pout.at[h, p], pin.at[h, p], sy_send.at[p, h], sy_recv.at[p, h], sibling
+        )
+
+    def ffn_down(p):
+        if p == 0:
+            down_load.wait()
+        for h in range(H):
+            for n in range(span // step):
+                cut = slice(n * step, (n + 1) * step)
+                full = slice(h * span + n * step, h * span + (n + 1) * step)
+                y = jnp.dot(hid[...], wd[:, full], preferred_element_type=f32).astype(bf16)
+                y = y.reshape(J, 2, C, step)
+                mine[h, p, :, :, cut] = y[:, 0]
+                pout[h, p, :, :, cut] = y[:, 1]
+            link.start(siby(p, h))
+
+    def back(p, j, h):
+        return link.copy(
+            mine.at[h, p, j],
+            ret.at[h, p, j],
+            rt_send.at[p, j - 1, h],
+            rt_recv.at[p, j - 1, h],
+            plane(j),
+        )
+
+    def give(p):
+        for h in range(H):
+            siby(p, h).wait_recv()
+            for j in range(J):
+                total = (mine[h, p, j].astype(f32) + pin[h, p, j].astype(f32)).astype(bf16)
+                if j == 0:
+                    ret[h, p, 0] = total
+                else:
+                    mine[h, p, j] = total
+            for j in (3, 1, 2):
+                link.start(back(p, j, h))
+
+    def zout(p, h):
+        return link.copy(
+            tout.at[h, p - 1], tin.at[h, z], zo_send.at[p - 1, h], zo_recv.at[z, h], at_z(zp[p])
+        )
+
+    def zin(p, h):
+        return link.copy(
+            tout.at[h, p - 1],
+            tin.at[h, zp[p]],
+            zo_send.at[p - 1, h],
+            zo_recv.at[zp[p], h],
+            at_z(zp[p]),
+        )
+
+    def mixed_part(p, h):
+        for j in (3, 1, 2):
+            back(p, j, h).wait_recv()
+        got = ret[h, p].reshape(J * C, span)
+        return jnp.dot(hi[p], got, preferred_element_type=f32) + jnp.dot(
+            lo[p], got, preferred_element_type=f32
+        )
+
+    def combine(p):
+        for h in range(H):
+            tout[h, p - 1] = mixed_part(p, h).astype(bf16)
+            link.start(zout(p, h))
+
+    for d in (0, 1):
+        link.start(tz(d, 1), inside(z + sign(d)))
+    select(0)
+    arrive(1)
+    select(1)
+    gather(0)
+    ffn_up(0)
+    ffn_down(0)
+    arrive(2)
+    select(2)
+    gather(1)
+    ffn_up(1)
+    ffn_down(1)
+    arrive(3)
+    select(3)
+    give(1)
+    gather(2)
+    ffn_up(2)
+    ffn_down(2)
+    gather(3)
+    ffn_up(3)
+    ffn_down(3)
+    give(3)
+    give(2)
+    give(0)
+    combine(1)
+    combine(3)
+    combine(2)
+    for h in range(H):
+        cut = slice(h * span, (h + 1) * span)
+        tot[:, cut] = res[:, cut].astype(f32) + mixed_part(0, h)
+    for h in range(H):
+        cut = slice(h * span, (h + 1) * span)
+        acc = tot[:, cut]
+        for p in range(1, Z):
+            zin(p, h).wait_recv()
+            acc = acc + tin[h, zp[p]].astype(f32)
+        out_ref[:, cut] = acc.astype(bf16)
+    link.drain()
+
+
+def fused(
+    conv_value, conv_gate, conv_taps, norm_gain, norm_bias, out_weight, stream,
+    routes, route_weights, expert_gain, gate_w, up_w, down_w,
+):
+    T = lax.axis_size("tp")
+    S, Z = lax.axis_size("sp"), T // 2
+    tokens, W = stream.shape
+    C = routes.shape[1] * tokens // S
+    F = gate_w.shape[2]
+    ch, run = conv_value.shape
+    taps_n = conv_taps.shape[1]
+    rim = -(-(taps_n - 1) // 16) * 16
+    tiles = F // 128
+    H = 2
+    span = W // H
+    f32, bf16 = jnp.float32, jnp.bfloat16
+    vmem = pl.BlockSpec(memory_space=pltpu.VMEM)
+    hbm = pl.BlockSpec(memory_space=pl.ANY)
+    dma = pltpu.SemaphoreType.DMA
+    rows = (H, Z, S, C, span)
+    return pl.pallas_call(
+        functools.partial(fused_kernel, T, C, taps_n),
+        out_shape=jax.ShapeDtypeStruct((tokens, W), bf16),
+        in_specs=[vmem] * 9 + [hbm] * 4,
+        out_specs=vmem,
+        scratch_shapes=[
+            pltpu.VMEM((rim + run, ch), f32),
+            pltpu.VMEM((rim, ch), bf16),
+            pltpu.VMEM((rim, ch), bf16),
+            pltpu.VMEM((T, tokens, ch), bf16),
+            pltpu.VMEM((T, tokens, ch), bf16),
+            pltpu.VMEM(out_weight.shape, bf16),
+            pltpu.VMEM((tokens, W), bf16),
+            pltpu.VMEM((Z, 8, 128), f32),
+            pltpu.VMEM((Z, S * C, tokens), bf16),
+            pltpu.VMEM((Z, tokens, S * C), bf16),
+            pltpu.VMEM((Z, tokens, S * C), bf16),
+            pltpu.VMEM((Z, tokens, W), bf16),
+            pltpu.VMEM((Z, S - 1, C, W), bf16),
+            pltpu.VMEM((Z, S, 2, C, W), bf16),
+            pltpu.VMEM((tiles, W, 256), bf16),
+            pltpu.VMEM((F, W), bf16),
+            pltpu.VMEM((S * 2 * C, F), bf16),
+            pltpu.VMEM(rows, bf16),
+            pltpu.VMEM(rows, bf16),
+            pltpu.VMEM(rows, bf16),
+            pltpu.VMEM(rows, bf16),
+            pltpu.VMEM((tokens, W), f32),
+            pltpu.VMEM((H, Z - 1, tokens, span), bf16),
+            pltpu.VMEM((H, Z, tokens, span), bf16),
+            dma((2 * tiles + 2,)),
+            dma((2,)),
+            dma((T - 1,)),
+            dma((T - 1,)),
+            dma((Z - 1,)),
+            dma((Z,)),
+            dma((2, Z - 1)),
+            dma((2, Z - 1)),
+            dma((Z, S - 1)),
+            dma((Z, S - 1)),
+            dma((Z, S)),
+            dma((Z, S)),
+            dma((Z, H)),
+            dma((Z, H)),
+            dma((Z, S - 1, H)),
+            dma((Z, S - 1, H)),
+            dma((Z - 1, H)),
+            dma((Z, H)),
+        ],
+        compiler_params=pltpu.CompilerParams(
+            collective_id=2, has_side_effects=True, vmem_limit_bytes=60 * 1024 * 1024
+        ),
+        name="fused_block",
+    )(
+        conv_value, conv_gate, conv_taps.T, norm_gain.reshape(1, -1), norm_bias.reshape(1, -1),
+        routes.T, route_weights.T, expert_gain.reshape(1, -1), stream,
+        out_weight, gate_w, up_w, down_w,
+    )
+
+
 def per_device(
     conv_value,
     conv_gate,
@@ -469,6 +982,12 @@
     expert_up,
     expert_down,
 ):
+    square_plane = lax.axis_size("sp") == 4 and lax.axis_size("tp") == 8
+    if square_plane and expert_gate.shape[2] % 128 == 0 and conv_value.shape[0] % 128 == 0:
+        return fused(
+            conv_value, conv_gate, conv_taps, norm_gain, norm_bias, out_weight, stream,
+            routes, route_weights, expert_gain, expert_gate, expert_up, expert_down,
+        )
     f32 = jnp.float32
     local_ch = conv_value.shape[0]
     run_len = conv_value.shape[1]

time: 114 us -> 79.1 us (0.69)
  Pallas kernels: 93.5 us -> 77.3 us
  other arithmetic: 7.15 us -> 0 us
  starting transfers between devices: 4.86 us -> 0 us
  matrix products: 3.37 us -> 0 us
  local copies, waits for them, and re-layouts: 4.5 us -> 1.67 us
    pallas_call x2 -> x1, Pallas kernels: 93.5 us -> 77.3 us  [fused(): pl.pallas_call(functools.partial(fused_kernel, T, C, taps_n), out_shape=j...]
    ppermute x1 -> x0, starting transfers between devices: 4.86 us -> none  [shifted(): lax.ppermute(value, axis, [(source, source + steps) for source in range(i...]
    dot_general x1 -> x0, matrix products: 3.37 us -> none  [per_device(): projected = jnp.dot(token_major, out_weight, preferred_element_type=f32)]
    transpose x1 -> x0, other arithmetic: 3.01 us -> none  [per_device(): pieces = exchange(conv_out.T.reshape(parts, tok_rows, local_ch))]
    reduce_sum x2 -> x0, other arithmetic: 2.13 us -> none  [the longest x1 1.11 us: per_device(): spread = jnp.mean((whole_conv - center) ** 2, axis=1, keepdims=True)]
    convert_element_type x3 -> x0, other arithmetic: 1.99 us -> none  [the longest x1 1.05 us: per_device(): (conv_value.astype(f32) * jax.nn.sigmoid(conv_gate.astype(f32))).astype(j...]
    mul x2 -> x0, local copies, waits for them, and re-layouts: 1.96 us -> none  [per_device(): conv_taps[:, offset:offset + 1] * padded[:, offset:offset + run_len]]
  transfers between devices with their start and end apart: 1 -> 0, of which waited for: 0 -> 0; matrix products, arithmetic and copies ran while one was open for 2% -> 0% of each run, Pallas kernels for 0% -> 0%
where the time goes in v1:
time: 79.1 us; the launch traced here: 79 us
  Pallas kernels  77.3 us (98%)
  local copies, waits for them, and re-layouts  1.67 us (2%)
    pallas_call x1, Pallas kernels, fused(): pl.pallas_call(functools.partial(fused_kernel, T, C, taps_n), out_shape=j...  77.3 us
    unnamed x1, local copies, waits for them, and re-layouts  1.67 us

profile of v1, /device:TPU:0, one launch (start us, length us, event | category | flops | bytes accessed | tf_op | source)
XLA Modules:
  0.0 79.0 jit_solution(8434140484914316188)
XLA Ops:
  0.0 77.3 %fused_block.1 = bf16[64,2048]{1,0:T(8,128)(2,1)} custom-call(bf16[128,512]{1,0:T(8,128)(2,1)} %value_ref.1, bf16[128,512]{1,0:T(8,128)(2,1)} %vgate_ref.1, f32[31,128]{1,0:T(8,128)} %bitcast.6, f32[1,1024]{1,0:T(1,128)} %bitcast.8, f32[1,1024]{1,0:T(1,128)} %bitcast.9, s32[2,64]{1,0:T(2,128)} %bitcast.10, f32[2,64]{1,0:T(2,128)} %bitcast.11, ...), custom_call_target="tpu_custom_call" | custom-call | tf_op jit(solution)/shard_map/fused_block/pallas_call | solution.py:910
  77.3 1.7 %copy.15 = bf16[64,2048]{1,0:T(8,128)(2,1)} copy(bf16[64,2048]{1,0:T(8,128)(2,1)} %fused_block.1) | data formatting | bytes 524288

commit v2 on v1

--- a/solution.py
+++ b/solution.py
@@ -525,6 +525,8 @@
     tot,
     tout,
     tin,
+    tmid,
+    rin,
     w_sem,
     halo_sem,
     ex_send,
@@ -543,6 +545,11 @@
     rt_recv,
     zo_send,
     zo_recv,
+    tm_recv,
+    cx_send,
+    cx_recv,
+    nr_send,
+    nr_recv,
 ):
     f32, bf16 = jnp.float32, jnp.bfloat16
     s = lax.axis_index("sp")
@@ -566,7 +573,8 @@
 
     sibling = (s, z * 2 + 1 - c)
 
-    zp = [z, 1 + z % 2, 2 + z // 2 - 2 * (z % 2), 3 - 3 * (z // 2)]
+    zp = [z, 1 + z % 2, 2 + z % 2 - 2 * (z // 2), 3 - 3 * (z % 2)]
+    middle = (z >= 1) & (z <= Z - 2)
 
     outw_load = pltpu.make_async_copy(outw_hbm, outw, w_sem.at[2 * tiles + 1])
     outw_load.start()
@@ -646,11 +654,12 @@
         exchanges.append(cp)
     land[t] = cbuf[t]
 
-    for i in range(1, Z):
-        zs = lax.rem(z + Z - i, Z)
+    metas = [
         link.copy(
-            meta.at[zs], meta.at[zs], meta_send.at[i - 1], meta_recv.at[zs], at_z(zs)
-        ).wait_recv()
+            meta.at[zp[p]], meta.at[zp[p]], meta_send.at[p - 1], meta_recv.at[zp[p]], at_z(zp[p])
+        )
+        for p in range(1, Z)
+    ]
 
     row = lax.broadcasted_iota(jnp.int32, (J, tokens), 0)
     ids = (((gy + (row >> 1)) & 1) * 2 + ((gx + (row & 1)) & 1)).astype(f32)
@@ -661,7 +670,9 @@
         0.0,
     ).astype(bf16)
     slot = lax.broadcasted_iota(jnp.int32, (C, tokens), 0).astype(f32)
-    for p in range(Z):
+    def matrices(p):
+        if p > 0:
+            metas[p - 1].wait_recv()
         m = meta[zp[p]]
         r0, r1 = m[0:1, :tokens], m[1:2, :tokens]
         w0, w1 = m[2:3, :tokens], m[3:4, :tokens]
@@ -679,6 +690,8 @@
         high = spread.astype(bf16)
         hi[p] = high
         lo[p] = (spread - high.astype(f32)).astype(bf16)
+
+    matrices(0)
 
     for cp in exchanges:
         cp.wait_recv()
@@ -706,97 +719,117 @@
         cut = slice(n * step, (n + 1) * step)
         tok[z, :, cut] = (res[:, cut].astype(f32) * scale * egain_ref[:, cut]).astype(bf16)
 
+    H = pout.shape[0]
+    span = W // H
+
+    def half(h):
+        return pl.ds(h * span, span)
+
     def sign(d):
         return 1 if d == 0 else -1
 
     def inside(v):
         return (v >= 0) & (v < Z)
 
-    def tz(d, k):
-        block = lax.rem(z - sign(d) * (k - 1) + Z, Z)
+    def tz(d, k, h, steps):
+        block = lax.rem(z - sign(d) * steps + Z, Z)
         return link.copy(
-            tok.at[block],
-            tok.at[block],
-            tz_send.at[d, k - 1],
-            tz_recv.at[d, k - 1],
+            tok.at[block, :, half(h)],
+            tok.at[block, :, half(h)],
+            tz_send.at[d, k - 1, h],
+            tz_recv.at[d, k - 1, h],
             at_z(lax.rem(z + sign(d) + Z, Z)),
         )
 
-    def tz_in(d, k):
-        block = lax.rem(z - sign(d) * k + Z, Z)
-        return link.copy(
-            tok.at[block],
-            tok.at[block],
-            tz_send.at[d, k - 1],
-            tz_recv.at[d, k - 1],
-            at_z(lax.rem(z + sign(d) + Z, Z)),
-        )
-
-    def arrive(k):
+    def arrive(k, h):
         for d in (0, 1):
             sg = sign(d)
-            pl.when(inside(z - sg * k))(tz_in(d, k).wait_recv)
+            pl.when(inside(z - sg * k))(tz(d, k, h, k).wait_recv)
             if k < Z - 1:
-                link.start(tz(d, k + 1), inside(z - sg * k) & inside(z + sg))
-
-    def pland(p, j):
+                link.start(tz(d, k + 1, h, k), inside(z - sg * k) & inside(z + sg))
+
+    def pland(p, j, h):
         return link.copy(
-            sbuf.at[p, j - 1], X.at[p, j, 0], pl_send.at[p, j - 1], pl_recv.at[p, j - 1], plane(j)
-        )
-
-    def sibx(p, j):
-        return link.copy(X.at[p, j, 0], X.at[p, j, 1], sx_send.at[p, j], sx_recv.at[p, j], sibling)
-
-    def select(p):
-        for n in range(W // step):
-            cut = slice(n * step, (n + 1) * step)
+            sbuf.at[p, j - 1, :, half(h)],
+            X.at[p, j, 0, :, half(h)],
+            pl_send.at[p, j - 1, h],
+            pl_recv.at[p, j - 1, h],
+            plane(j),
+        )
+
+    def sibx(p, j, h):
+        return link.copy(
+            X.at[p, j, 0, :, half(h)],
+            X.at[p, j, 1, :, half(h)],
+            sx_send.at[p, j, h],
+            sx_recv.at[p, j, h],
+            sibling,
+        )
+
+    def select(p, h):
+        for n in range(span // step):
+            cut = slice(h * span + n * step, h * span + (n + 1) * step)
             sel = jnp.dot(cho[p], tok[zp[p], :, cut], preferred_element_type=f32).astype(bf16)
             X[p, 0, 0, :, cut] = sel[0:C]
             for j in range(1, J):
                 sbuf[p, j - 1, :, cut] = sel[j * C : (j + 1) * C]
+        for j in (1, 2) if p == 1 else (3, 1, 2):
+            link.start(pland(p, j, h))
+        link.start(sibx(p, 0, h))
+
+    def corner(d, h):
+        return link.copy(
+            X.at[0, 3, 0, :, half(h)],
+            X.at[1, 3, 0, :, half(h)],
+            cx_send.at[d, h],
+            cx_recv.at[h],
+            at_z(lax.rem(z + sign(d) + Z, Z)),
+        )
+
+    def forward(p, h):
         for j in (3, 1, 2):
-            link.start(pland(p, j))
-        link.start(sibx(p, 0))
+            if p == 1 and j == 3:
+                corner(0, h).wait_recv()
+            else:
+                pland(p, j, h).wait_recv()
+            link.start(sibx(p, j, h))
+            if p == 0 and j == 3:
+                for d in (0, 1):
+                    link.start(corner(d, h), middle)
 
     def gather(p):
-        for j in (3, 1, 2):
-            pland(p, j).wait_recv()
-            link.start(sibx(p, j))
-        for j in range(J):
-            sibx(p, j).wait_recv()
+        for h in range(H):
+            for j in range(J):
+                sibx(p, j, h).wait_recv()
 
     M = J * 2 * C
 
-    def ffn_up(p):
-        if p == 0:
+    def ffn_up(p, start=0, stop=tiles):
+        if p == 0 and start == 0:
             for cp in loads:
                 cp.wait()
-        for j in range(tiles):
+        for j in range(start, stop):
             x = X[p].reshape(M, W)
             both = jnp.dot(x, wg[j], preferred_element_type=f32)
             g, u = both[:, :128], both[:, 128:]
             hid[:, j * 128 : (j + 1) * 128] = (jax.nn.silu(g) * u).astype(bf16)
 
-    H = pout.shape[0]
-    span = W // H
-
     def siby(p, h):
         return link.copy(
             pout.at[h, p], pin.at[h, p], sy_send.at[p, h], sy_recv.at[p, h], sibling
         )
 
-    def ffn_down(p):
-        if p == 0:
+    def ffn_down(p, h):
+        if p == 0 and h == 0:
             down_load.wait()
-        for h in range(H):
-            for n in range(span // step):
-                cut = slice(n * step, (n + 1) * step)
-                full = slice(h * span + n * step, h * span + (n + 1) * step)
-                y = jnp.dot(hid[...], wd[:, full], preferred_element_type=f32).astype(bf16)
-                y = y.reshape(J, 2, C, step)
-                mine[h, p, :, :, cut] = y[:, 0]
-                pout[h, p, :, :, cut] = y[:, 1]
-            link.start(siby(p, h))
+        for n in range(span // step):
+            cut = slice(n * step, (n + 1) * step)
+            full = slice(h * span + n * step, h * span + (n + 1) * step)
+            y = jnp.dot(hid[...], wd[:, full], preferred_element_type=f32).astype(bf16)
+            y = y.reshape(J, 2, C, step)
+            mine[h, p, :, :, cut] = y[:, 0]
+            pout[h, p, :, :, cut] = y[:, 1]
+        link.start(siby(p, h))
 
     def back(p, j, h):
         return link.copy(
@@ -807,30 +840,49 @@
             plane(j),
         )
 
-    def give(p):
-        for h in range(H):
-            siby(p, h).wait_recv()
-            for j in range(J):
-                total = (mine[h, p, j].astype(f32) + pin[h, p, j].astype(f32)).astype(bf16)
-                if j == 0:
-                    ret[h, p, 0] = total
-                else:
-                    mine[h, p, j] = total
-            for j in (3, 1, 2):
-                link.start(back(p, j, h))
+    def neighbour_rows(spot, h):
+        return link.copy(
+            mine.at[h, 1], rin.at[spot, h], nr_send.at[h], nr_recv.at[spot, h], at_z(zp[1])
+        )
+
+    def give(p, h):
+        siby(p, h).wait_recv()
+        total = mine[h, p].astype(f32) + pin[h, p].astype(f32)
+        if p == 1:
+            mine[h, 1] = total.astype(bf16)
+            link.start(neighbour_rows(z // 2, h))
+            return
+        if p == 0:
+
+            @pl.when(middle)
+            def _():
+                neighbour_rows(0, h).wait_recv()
+                neighbour_rows(1, h).wait_recv()
+                mine[h, 0] = (total + rin[0, h].astype(f32) + rin[1, h].astype(f32)).astype(bf16)
+
+            @pl.when(jnp.logical_not(middle))
+            def _():
+                mine[h, 0] = total.astype(bf16)
+
+        else:
+            mine[h, p] = total.astype(bf16)
+        ret[h, p, 0] = mine[h, p, 0]
+        for j in (3, 1, 2):
+            link.start(back(p, j, h))
 
     def zout(p, h):
         return link.copy(
-            tout.at[h, p - 1], tin.at[h, z], zo_send.at[p - 1, h], zo_recv.at[z, h], at_z(zp[p])
+            tout.at[h, p - 2], tin.at[h, z], zo_send.at[p - 2, h], zo_recv.at[z, h], at_z(zp[p])
         )
 
     def zin(p, h):
         return link.copy(
-            tout.at[h, p - 1],
-            tin.at[h, zp[p]],
-            zo_send.at[p - 1, h],
-            zo_recv.at[zp[p], h],
-            at_z(zp[p]),
+            tout.at[h, 0], tin.at[h, zp[p]], zo_send.at[0, h], zo_recv.at[zp[p], h], at_z(zp[p])
+        )
+
+    def zmid(h):
+        return link.copy(
+            tout.at[h, 1], tmid.at[h], zo_send.at[1, h], tm_recv.at[h], at_z(zp[1])
         )
 
     def mixed_part(p, h):
@@ -841,49 +893,99 @@
             lo[p], got, preferred_element_type=f32
         )
 
-    def combine(p):
-        for h in range(H):
-            tout[h, p - 1] = mixed_part(p, h).astype(bf16)
-            link.start(zout(p, h))
-
-    for d in (0, 1):
-        link.start(tz(d, 1), inside(z + sign(d)))
-    select(0)
-    arrive(1)
-    select(1)
+    end = jnp.logical_not(middle)
+
+    def combine(p, h):
+        tout[h, p - 2] = mixed_part(p, h).astype(bf16)
+        if p == 2:
+            link.start(zout(2, h), end)
+        else:
+            link.start(zmid(h), end)
+            link.start(zout(3, h), middle)
+
+    def merge(h):
+        @pl.when(middle)
+        def _():
+            zmid(h).wait_recv()
+            tout[h, 0] = (tout[h, 0].astype(f32) + tmid[h].astype(f32)).astype(bf16)
+
+        link.start(zout(2, h), middle)
+
+    for h in range(H):
+        for d in (0, 1):
+            link.start(tz(d, 1, h, 0), inside(z + sign(d)))
+    select(0, 0)
+    select(0, 1)
+    matrices(1)
+    matrices(2)
+    matrices(3)
+    arrive(1, 0)
+    select(1, 0)
+    forward(0, 0)
+    arrive(1, 1)
+    select(1, 1)
+    forward(0, 1)
     gather(0)
     ffn_up(0)
-    ffn_down(0)
-    arrive(2)
-    select(2)
+    arrive(2, 0)
+    select(2, 0)
+    forward(1, 0)
+    ffn_down(0, 0)
+    arrive(2, 1)
+    select(2, 1)
+    ffn_down(0, 1)
+    forward(1, 1)
     gather(1)
+    arrive(3, 0)
+    select(3, 0)
     ffn_up(1)
-    ffn_down(1)
-    arrive(3)
-    select(3)
-    give(1)
+    arrive(3, 1)
+    select(3, 1)
+    forward(2, 0)
+    ffn_down(1, 0)
+    forward(2, 1)
+    ffn_down(1, 1)
     gather(2)
+    give(1, 0)
+    give(1, 1)
     ffn_up(2)
-    ffn_down(2)
+    forward(3, 0)
+    ffn_down(2, 0)
+    forward(3, 1)
+    ffn_down(2, 1)
+    give(2, 0)
     gather(3)
-    ffn_up(3)
-    ffn_down(3)
-    give(3)
-    give(2)
-    give(0)
-    combine(1)
-    combine(3)
-    combine(2)
+    ffn_up(3, 0, tiles // 2)
+    give(2, 1)
+    ffn_up(3, tiles // 2, tiles)
+    ffn_down(3, 0)
+    ffn_down(3, 1)
+    give(3, 0)
+    combine(2, 0)
+    combine(2, 1)
+    give(3, 1)
+    combine(3, 0)
+    give(0, 0)
+    combine(3, 1)
+    give(0, 1)
     for h in range(H):
+        merge(h)
         cut = slice(h * span, (h + 1) * span)
         tot[:, cut] = res[:, cut].astype(f32) + mixed_part(0, h)
     for h in range(H):
         cut = slice(h * span, (h + 1) * span)
-        acc = tot[:, cut]
-        for p in range(1, Z):
-            zin(p, h).wait_recv()
-            acc = acc + tin[h, zp[p]].astype(f32)
-        out_ref[:, cut] = acc.astype(bf16)
+        zin(2, h).wait_recv()
+        acc = tot[:, cut] + tin[h, zp[2]].astype(f32)
+
+        @pl.when(middle)
+        def _():
+            out_ref[:, cut] = acc.astype(bf16)
+
+        @pl.when(end)
+        def _():
+            zin(1, h).wait_recv()
+            out_ref[:, cut] = (acc + tin[h, zp[1]].astype(f32)).astype(bf16)
+
     link.drain()
 
 
@@ -935,26 +1037,33 @@
             pltpu.VMEM(rows, bf16),
             pltpu.VMEM(rows, bf16),
             pltpu.VMEM((tokens, W), f32),
-            pltpu.VMEM((H, Z - 1, tokens, span), bf16),
+            pltpu.VMEM((H, 2, tokens, span), bf16),
             pltpu.VMEM((H, Z, tokens, span), bf16),
+            pltpu.VMEM((H, tokens, span), bf16),
+            pltpu.VMEM((2, H, S, C, span), bf16),
             dma((2 * tiles + 2,)),
             dma((2,)),
             dma((T - 1,)),
             dma((T - 1,)),
             dma((Z - 1,)),
             dma((Z,)),
-            dma((2, Z - 1)),
-            dma((2, Z - 1)),
-            dma((Z, S - 1)),
-            dma((Z, S - 1)),
-            dma((Z, S)),
-            dma((Z, S)),
+            dma((2, Z - 1, H)),
+            dma((2, Z - 1, H)),
+            dma((Z, S - 1, H)),
+            dma((Z, S - 1, H)),
+            dma((Z, S, H)),
+            dma((Z, S, H)),
             dma((Z, H)),
             dma((Z, H)),
             dma((Z, S - 1, H)),
             dma((Z, S - 1, H)),
-            dma((Z - 1, H)),
+            dma((2, H)),
             dma((Z, H)),
+            dma((H,)),
+            dma((2, H)),
+            dma((H,)),
+            dma((H,)),
+            dma((2, H)),
         ],
         compiler_params=pltpu.CompilerParams(
             collective_id=2, has_side_effects=True, vmem_limit_bytes=60 * 1024 * 1024

time: 79.1 us -> 73.1 us (0.924)
  Pallas kernels: 77.3 us -> 71.2 us
    pallas_call x1, Pallas kernels: 77.3 us -> 71.2 us  [fused(): pl.pallas_call(functools.partial(fused_kernel, T, C, taps_n), out_shape=j...]
where the time goes in v2:
time: 73.1 us; the launch traced here: 72.9 us
  Pallas kernels  71.2 us (97%)
  local copies, waits for them, and re-layouts  1.67 us (2%)
    pallas_call x1, Pallas kernels, fused(): pl.pallas_call(functools.partial(fused_kernel, T, C, taps_n), out_shape=j...  71.2 us
    unnamed x1, local copies, waits for them, and re-layouts  1.67 us

profile of v2, /device:TPU:0, one launch (start us, length us, event | category | flops | bytes accessed | tf_op | source)
XLA Modules:
  0.0 72.9 jit_solution(4835694099296200915)
XLA Ops:
  0.0 71.2 %fused_block.1 = bf16[64,2048]{1,0:T(8,128)(2,1)} custom-call(bf16[128,512]{1,0:T(8,128)(2,1)} %value_ref.1, bf16[128,512]{1,0:T(8,128)(2,1)} %vgate_ref.1, f32[31,128]{1,0:T(8,128)} %bitcast.6, f32[1,1024]{1,0:T(1,128)} %bitcast.8, f32[1,1024]{1,0:T(1,128)} %bitcast.9, s32[2,64]{1,0:T(2,128)} %bitcast.10, f32[2,64]{1,0:T(2,128)} %bitcast.11, ...), custom_call_target="tpu_custom_call" | custom-call | tf_op jit(solution)/shard_map/fused_block/pallas_call | solution.py:1012
  71.2 1.7 %copy.15 = bf16[64,2048]{1,0:T(8,128)(2,1)} copy(bf16[64,2048]{1,0:T(8,128)(2,1)} %fused_block.1) | data formatting | bytes 524288

commit v3 on v2

--- a/solution.py
+++ b/solution.py
@@ -487,20 +487,24 @@
     T,
     C,
     taps_n,
-    value_ref,
-    vgate_ref,
+    H,
+    value_hbm,
+    vgate_hbm,
     taps_ref,
     gain_ref,
     bias_ref,
     routes_ref,
     weights_ref,
     egain_ref,
-    stream_ref,
+    stream_hbm,
     outw_hbm,
     gate_hbm,
     up_hbm,
     down_hbm,
     out_ref,
+    value_ref,
+    vgate_ref,
+    stream_ref,
     gbuf,
     halo_out,
     halo_in,
@@ -546,8 +550,6 @@
     zo_send,
     zo_recv,
     tm_recv,
-    cx_send,
-    cx_recv,
     nr_send,
     nr_recv,
 ):
@@ -576,6 +578,14 @@
     zp = [z, 1 + z % 2, 2 + z % 2 - 2 * (z // 2), 3 - 3 * (z % 2)]
     middle = (z >= 1) & (z <= Z - 2)
 
+    early = [
+        pltpu.make_async_copy(src, dst, w_sem.at[2 * tiles + 2 + i])
+        for i, (src, dst) in enumerate(
+            ((value_hbm, value_ref), (vgate_hbm, vgate_ref), (stream_hbm, stream_ref))
+        )
+    ]
+    for cp in early:
+        cp.start()
     outw_load = pltpu.make_async_copy(outw_hbm, outw, w_sem.at[2 * tiles + 1])
     outw_load.start()
     loads = []
@@ -598,6 +608,8 @@
     for peer in peers:
         pl.semaphore_signal(barrier, inc=1, device_id=peer, device_id_type=MESH)
 
+    early[0].wait()
+    early[1].wait()
     gated = (
         value_ref[...].astype(f32) * jax.nn.sigmoid(vgate_ref[...].astype(f32))
     ).astype(bf16)
@@ -703,6 +715,7 @@
         whole * lax.rsqrt(var + epsilon) * gain_ref[...] + bias_ref[...]
     ).astype(bf16)
     outw_load.wait()
+    early[2].wait()
     step = 512
     square = jnp.zeros((tokens, 1), f32)
     for n in range(W // step):
@@ -719,8 +732,8 @@
         cut = slice(n * step, (n + 1) * step)
         tok[z, :, cut] = (res[:, cut].astype(f32) * scale * egain_ref[:, cut]).astype(bf16)
 
-    H = pout.shape[0]
-    span = W // H
+    R = pout.shape[0]
+    span, part = W // H, W // R
 
     def half(h):
         return pl.ds(h * span, span)
@@ -773,29 +786,14 @@
             X[p, 0, 0, :, cut] = sel[0:C]
             for j in range(1, J):
                 sbuf[p, j - 1, :, cut] = sel[j * C : (j + 1) * C]
-        for j in (1, 2) if p == 1 else (3, 1, 2):
+        for j in (3, 1, 2):
             link.start(pland(p, j, h))
         link.start(sibx(p, 0, h))
 
-    def corner(d, h):
-        return link.copy(
-            X.at[0, 3, 0, :, half(h)],
-            X.at[1, 3, 0, :, half(h)],
-            cx_send.at[d, h],
-            cx_recv.at[h],
-            at_z(lax.rem(z + sign(d) + Z, Z)),
-        )
-
     def forward(p, h):
         for j in (3, 1, 2):
-            if p == 1 and j == 3:
-                corner(0, h).wait_recv()
-            else:
-                pland(p, j, h).wait_recv()
+            pland(p, j, h).wait_recv()
             link.start(sibx(p, j, h))
-            if p == 0 and j == 3:
-                for d in (0, 1):
-                    link.start(corner(d, h), middle)
 
     def gather(p):
         for h in range(H):
@@ -822,9 +820,9 @@
     def ffn_down(p, h):
         if p == 0 and h == 0:
             down_load.wait()
-        for n in range(span // step):
+        for n in range(part // step):
             cut = slice(n * step, (n + 1) * step)
-            full = slice(h * span + n * step, h * span + (n + 1) * step)
+            full = slice(h * part + n * step, h * part + (n + 1) * step)
             y = jnp.dot(hid[...], wd[:, full], preferred_element_type=f32).astype(bf16)
             y = y.reshape(J, 2, C, step)
             mine[h, p, :, :, cut] = y[:, 0]
@@ -888,7 +886,7 @@
     def mixed_part(p, h):
         for j in (3, 1, 2):
             back(p, j, h).wait_recv()
-        got = ret[h, p].reshape(J * C, span)
+        got = ret[h, p].reshape(J * C, part)
         return jnp.dot(hi[p], got, preferred_element_type=f32) + jnp.dot(
             lo[p], got, preferred_element_type=f32
         )
@@ -925,15 +923,21 @@
     arrive(1, 1)
     select(1, 1)
     forward(0, 1)
+    first, second = range(R // 2), range(R // 2, R)
+
+    def each(f, p, pieces):
+        for q in pieces:
+            f(p, q)
+
     gather(0)
     ffn_up(0)
     arrive(2, 0)
     select(2, 0)
     forward(1, 0)
-    ffn_down(0, 0)
+    each(ffn_down, 0, first)
     arrive(2, 1)
     select(2, 1)
-    ffn_down(0, 1)
+    each(ffn_down, 0, second)
     forward(1, 1)
     gather(1)
     arrive(3, 0)
@@ -942,40 +946,38 @@
     arrive(3, 1)
     select(3, 1)
     forward(2, 0)
-    ffn_down(1, 0)
+    each(ffn_down, 1, first)
     forward(2, 1)
-    ffn_down(1, 1)
+    each(ffn_down, 1, second)
     gather(2)
-    give(1, 0)
-    give(1, 1)
+    each(give, 1, range(R))
     ffn_up(2)
     forward(3, 0)
-    ffn_down(2, 0)
+    each(ffn_down, 2, first)
     forward(3, 1)
-    ffn_down(2, 1)
-    give(2, 0)
+    each(ffn_down, 2, second)
+    each(give, 2, first)
     gather(3)
     ffn_up(3, 0, tiles // 2)
-    give(2, 1)
+    each(give, 2, second)
     ffn_up(3, tiles // 2, tiles)
-    ffn_down(3, 0)
-    ffn_down(3, 1)
-    give(3, 0)
-    combine(2, 0)
-    combine(2, 1)
-    give(3, 1)
-    combine(3, 0)
-    give(0, 0)
-    combine(3, 1)
-    give(0, 1)
-    for h in range(H):
-        merge(h)
-        cut = slice(h * span, (h + 1) * span)
-        tot[:, cut] = res[:, cut].astype(f32) + mixed_part(0, h)
-    for h in range(H):
-        cut = slice(h * span, (h + 1) * span)
-        zin(2, h).wait_recv()
-        acc = tot[:, cut] + tin[h, zp[2]].astype(f32)
+    each(ffn_down, 3, range(R))
+    each(give, 3, first)
+    each(combine, 2, first)
+    for q in first:
+        give(3, R // 2 + q)
+        combine(2, R // 2 + q)
+    for q in range(R):
+        combine(3, q)
+        give(0, q)
+    for q in range(R):
+        merge(q)
+        cut = slice(q * part, (q + 1) * part)
+        tot[:, cut] = res[:, cut].astype(f32) + mixed_part(0, q)
+    for q in range(R):
+        cut = slice(q * part, (q + 1) * part)
+        zin(2, q).wait_recv()
+        acc = tot[:, cut] + tin[q, zp[2]].astype(f32)
 
         @pl.when(middle)
         def _():
@@ -983,8 +985,8 @@
 
         @pl.when(end)
         def _():
-            zin(1, h).wait_recv()
-            out_ref[:, cut] = (acc + tin[h, zp[1]].astype(f32)).astype(bf16)
+            zin(1, q).wait_recv()
+            out_ref[:, cut] = (acc + tin[q, zp[1]].astype(f32)).astype(bf16)
 
     link.drain()
 
@@ -1002,19 +1004,22 @@
     taps_n = conv_taps.shape[1]
     rim = -(-(taps_n - 1) // 16) * 16
     tiles = F // 128
-    H = 2
-    span = W // H
+    H, R = 2, 4
+    part = W // R
     f32, bf16 = jnp.float32, jnp.bfloat16
     vmem = pl.BlockSpec(memory_space=pltpu.VMEM)
     hbm = pl.BlockSpec(memory_space=pl.ANY)
     dma = pltpu.SemaphoreType.DMA
-    rows = (H, Z, S, C, span)
+    rows = (R, Z, S, C, part)
     return pl.pallas_call(
-        functools.partial(fused_kernel, T, C, taps_n),
+        functools.partial(fused_kernel, T, C, taps_n, H),
         out_shape=jax.ShapeDtypeStruct((tokens, W), bf16),
-        in_specs=[vmem] * 9 + [hbm] * 4,
+        in_specs=[hbm] * 2 + [vmem] * 6 + [hbm] * 5,
         out_specs=vmem,
         scratch_shapes=[
+            pltpu.VMEM((ch, run), bf16),
+            pltpu.VMEM((ch, run), bf16),
+            pltpu.VMEM((tokens, W), bf16),
             pltpu.VMEM((rim + run, ch), f32),
             pltpu.VMEM((rim, ch), bf16),
             pltpu.VMEM((rim, ch), bf16),
@@ -1037,11 +1042,11 @@
             pltpu.VMEM(rows, bf16),
             pltpu.VMEM(rows, bf16),
             pltpu.VMEM((tokens, W), f32),
-            pltpu.VMEM((H, 2, tokens, span), bf16),
-            pltpu.VMEM((H, Z, tokens, span), bf16),
-            pltpu.VMEM((H, tokens, span), bf16),
-            pltpu.VMEM((2, H, S, C, span), bf16),
-            dma((2 * tiles + 2,)),
+            pltpu.VMEM((R, 2, tokens, part), bf16),
+            pltpu.VMEM((R, Z, tokens, part), bf16),
+            pltpu.VMEM((R, tokens, part), bf16),
+            pltpu.VMEM((2, R, S, C, part), bf16),
+            dma((2 * tiles + 5,)),
             dma((2,)),
             dma((T - 1,)),
             dma((T - 1,)),
@@ -1053,17 +1058,15 @@
             dma((Z, S - 1, H)),
             dma((Z, S, H)),
             dma((Z, S, H)),
-            dma((Z, H)),
-            dma((Z, H)),
-            dma((Z, S - 1, H)),
-            dma((Z, S - 1, H)),
-            dma((2, H)),
-            dma((Z, H)),
-            dma((H,)),
-            dma((2, H)),
-            dma((H,)),
-            dma((H,)),
-            dma((2, H)),
+            dma((Z, R)),
+            dma((Z, R)),
+            dma((Z, S - 1, R)),
+            dma((Z, S - 1, R)),
+            dma((2, R)),
+            dma((Z, R)),
+            dma((R,)),
+            dma((R,)),
+            dma((2, R)),
         ],
         compiler_params=pltpu.CompilerParams(
             collective_id=2, has_side_effects=True, vmem_limit_bytes=60 * 1024 * 1024

time: 73.1 us -> 71.2 us (0.974)
  Pallas kernels: 71.2 us -> 69.3 us
    pallas_call x1, Pallas kernels: 71.2 us -> 69.3 us  [fused(): pl.pallas_call(functools.partial(fused_kernel, T, C, taps_n, H), out_shap...]
where the time goes in v3:
time: 71.2 us; the launch traced here: 71 us
  Pallas kernels  69.3 us (97%)
  local copies, waits for them, and re-layouts  1.67 us (2%)
    pallas_call x1, Pallas kernels, fused(): pl.pallas_call(functools.partial(fused_kernel, T, C, taps_n, H), out_shap...  69.3 us
    unnamed x1, local copies, waits for them, and re-layouts  1.67 us

profile of v3, /device:TPU:0, one launch (start us, length us, event | category | flops | bytes accessed | tf_op | source)
XLA Modules:
  0.0 71.0 jit_solution(12773332347262217102)
XLA Ops:
  0.0 69.3 %fused_block.1 = bf16[64,2048]{1,0:T(8,128)(2,1)} custom-call(bf16[128,512]{1,0:T(8,128)(2,1)} %value_hbm.1, bf16[128,512]{1,0:T(8,128)(2,1)} %vgate_hbm.1, f32[31,128]{1,0:T(8,128)} %bitcast.6, f32[1,1024]{1,0:T(1,128)} %bitcast.8, f32[1,1024]{1,0:T(1,128)} %bitcast.9, s32[2,64]{1,0:T(2,128)} %bitcast.10, f32[2,64]{1,0:T(2,128)} %bitcast.11, ...), custom_call_target="tpu_custom_call" | custom-call | tf_op jit(solution)/shard_map/fused_block/pallas_call | solution.py:1014
  69.3 1.7 %copy.15 = bf16[64,2048]{1,0:T(8,128)(2,1)} copy(bf16[64,2048]{1,0:T(8,128)(2,1)} %fused_block.1) | data formatting | bytes 524288
